TPU v7x, 32 devices: a whole 2x2x4 slice. The times are simulated.
32 devices in a mesh: ep: 8 (over z, x), tp: 4 (over y, core).
Axes of the slice: x: 2, y: 2, z: 4, core: 2. Of those that a mesh axis runs over, the one named last changes fastest.
Arguments:
- mixer_rows: bfloat16 [1024, 2048], P('ep'), may hold values from -40 to 40
- mixer_gain: float32 [2048], replicated, may hold values from 0.1 to 1.9
- inner_weight: bfloat16 [2048, 1024], P(None, 'tp'), may hold values from -0.125 to 0.125
- gate_in_weight: bfloat16 [2048, 1024], P(None, 'tp'), may hold values from -0.125 to 0.125
- gate_out_weight: bfloat16 [2048, 1024], P(None, 'tp'), may hold values from -0.125 to 0.125
- conv_taps: float32 [3, 1024], P(None, 'tp'), may hold values from -3.5 to 3.5
- mixer_out_weight: bfloat16 [1024, 2048], P('tp'), may hold values from -0.1875 to 0.1875
- routed_rows: bfloat16 [2048, 2048], P('ep'), may hold values from -40 to 40
- routed_gain: float32 [2048], replicated, may hold values from 0.1 to 1.9
- route_ids: int32 [2048, 2], P('ep'), may hold values from 0 to 7, all different within a row; in each aligned block of 256 rows (0 to 255, 256 to 511, ...) at most 128 rows name the same one
- route_weights: float32 [2048, 2], P('ep'), may hold values from 0.25 to 1
- expert_gate: bfloat16 [8, 2048, 2048], P('ep', None, 'tp'), may hold values from -0.125 to 0.125
- expert_up: bfloat16 [8, 2048, 2048], P('ep', None, 'tp'), may hold values from -0.125 to 0.125
- expert_down: bfloat16 [8, 2048, 2048], P('ep', 'tp'), may hold values from -0.125 to 0.125
Outputs:
- mixer_output: bfloat16 [1024, 2048], P('ep')
- routed_output: bfloat16 [2048, 2048], P('ep')
Inputs may be any that keep to these rules, and one draw needn't show every extreme that they name: `route_ids`: within each aligned block of 256 tokens, no expert is named by more than 128 choices, a bound that some block reaches; a token's 2 experts differ.
All inputs are finite; a program needn't handle non-finite values.
Results may differ from a plain program's by a relative error of at most 0.019.
Values may be sent and summed in bfloat16 or wider, within the bound.
A program may use at most 64 MiB of HBM per device.

v0:
```python
import jax
import jax.numpy as jnp
from jax import lax
from jax.sharding import PartitionSpec as P


def shifted(value, axis, steps):
    count = lax.axis_size(axis)
    initial, last = (max(0, -steps), min(count, count - steps))
    return lax.ppermute(value, axis, [(source, source + steps) for source in range(initial, last)])


def rms_scale(row_block, gain_row):
    values = row_block.astype(jnp.float32)
    scaled = values * lax.rsqrt(jnp.mean(values * values, axis=-1, keepdims=True) + 1e-06)
    return (scaled * gain_row).astype(jnp.bfloat16)


def on_device(
    mixer_rows,
    mixer_gain,
    inner_weight,
    gate_in_weight,
    gate_out_weight,
    conv_taps,
    mixer_out_weight,
    routed_rows,
    routed_gain,
    route_ids,
    route_weights,
    expert_gate,
    expert_up,
    expert_down,
):
    normed = rms_scale(mixer_rows, mixer_gain)
    inner_proj = jnp.dot(normed, inner_weight, preferred_element_type=jnp.float32)
    gate_in = jnp.dot(normed, gate_in_weight, preferred_element_type=jnp.float32)
    conv_input = (gate_in * inner_proj).astype(jnp.bfloat16)
    gate_out = jnp.dot(normed, gate_out_weight, preferred_element_type=jnp.float32)
    tap_total = conv_taps.shape[0]
    rim_rows = tap_total - 1
    earlier_rows = shifted(conv_input[conv_input.shape[0] - rim_rows :], "ep", 1)
    extended = jnp.concatenate([earlier_rows, conv_input], axis=0).astype(jnp.float32)
    length = conv_input.shape[0]
    conv_out = jnp.zeros(conv_input.shape, jnp.float32)
    for tap_index in range(tap_total):
        conv_out = conv_out + conv_taps[tap_index] * extended[tap_index : tap_index + length]
    gated_conv = (gate_out * conv_out).astype(jnp.bfloat16)
    mixer_terms = jnp.dot(gated_conv, mixer_out_weight, preferred_element_type=jnp.float32)
    routed_normed = rms_scale(routed_rows, routed_gain)
    experts = lax.axis_size("ep")
    groups = lax.axis_size("tp")
    column = lax.axis_index("tp")
    tok_count, pick_count = route_ids.shape
    model_width = routed_rows.shape[1]
    capacity = 2 * tok_count * pick_count // experts
    share_rows = capacity // groups
    flat_ids = route_ids.reshape(-1)
    onehot = (flat_ids[:, None] == jnp.arange(experts, dtype=jnp.int32)[None, :]).astype(jnp.int32)
    slot_rank = jnp.sum((jnp.cumsum(onehot, axis=0) - onehot) * onehot, axis=1)
    slot_number = slot_rank * experts + flat_ids
    owners = jnp.arange(tok_count * pick_count, dtype=jnp.int32) // pick_count
    matches = slot_number[None, :] == jnp.arange(capacity * experts, dtype=jnp.int32)[:, None]
    token_table = jnp.where(
        jnp.any(matches, axis=1), jnp.sum(jnp.where(matches, owners[None, :], 0), axis=1), tok_count
    )
    padded_rows = jnp.concatenate(
        [routed_normed, jnp.zeros((1, model_width), jnp.bfloat16)], axis=0
    )
    table_share = lax.dynamic_slice_in_dim(
        token_table.reshape(capacity, experts), column * share_rows, share_rows, 0
    )
    outgoing = jnp.take(padded_rows, table_share.reshape(-1), axis=0).reshape(
        share_rows, experts, model_width
    )
    arrived = lax.all_to_all(outgoing, "ep", split_axis=1, concat_axis=1, tiled=True)
    incoming = lax.all_gather(arrived, "tp", axis=0, tiled=True)
    slot_rows = incoming.reshape(capacity * experts, model_width)
    gate_act = jnp.dot(slot_rows, expert_gate[0], preferred_element_type=jnp.float32)
    up_act = jnp.dot(slot_rows, expert_up[0], preferred_element_type=jnp.float32)
    hidden = (jax.nn.silu(gate_act) * up_act).astype(jnp.bfloat16)
    summed = lax.psum_scatter(
        jnp.dot(hidden, expert_down[0], preferred_element_type=jnp.float32).astype(jnp.bfloat16),
        "tp",
        scatter_dimension=0,
        tiled=True,
    )
    returned = lax.all_to_all(
        summed.reshape(share_rows, experts, model_width),
        "ep",
        split_axis=1,
        concat_axis=1,
        tiled=True,
    )
    flat_back = jnp.concatenate(
        [
            returned.reshape(share_rows * experts, model_width),
            jnp.zeros((1, model_width), jnp.bfloat16),
        ],
        axis=0,
    )
    local_slot = jnp.where(
        slot_rank // share_rows == column,
        (slot_rank - column * share_rows) * experts + flat_ids,
        share_rows * experts,
    )
    contrib = (
        jnp.take(flat_back, local_slot, axis=0).astype(jnp.float32)
        * route_weights.reshape(-1)[:, None]
    )
    routed_terms = jnp.sum(contrib.reshape(tok_count, pick_count, model_width), axis=1)
    mixer_total, routed_total = (
        lax.psum(mixer_terms.astype(jnp.bfloat16), "tp").astype(jnp.float32),
        lax.psum(routed_terms.astype(jnp.bfloat16), "tp").astype(jnp.float32),
    )
    return (mixer_total.astype(jnp.bfloat16), routed_total.astype(jnp.bfloat16))


def solution(mesh):
    return jax.shard_map(
        on_device,
        mesh=mesh,
        in_specs=(
            P("ep", None),
            P(),
            P(None, "tp"),
            P(None, "tp"),
            P(None, "tp"),
            P(None, "tp"),
            P("tp", None),
            P("ep", None),
            P(),
            P("ep", None),
            P("ep", None),
            P("ep", None, "tp"),
            P("ep", None, "tp"),
            P("ep", "tp", None),
        ),
        out_specs=(P("ep", None), P("ep", None)),
        check_vma=False,
    )
```

profile of v0, /device:TPU:0, one launch (start us, length us, event | category | flops | bytes accessed | tf_op | source)
XLA Modules:
  0.0 255.2 jit_solution(8111063935972421025)
XLA Ops:
  7.2 0.0 copy-start
  7.2 0.0 copy-start.1
  7.2 0.0 all-gather.2.cloned.1.call-start
  7.2 1.0 copy.67
  8.2 0.1 eq.62
  8.4 0.1 eq.58
  8.5 1.1 reduce-window.6
  9.7 0.2 slice_reduce_fusion
  9.9 0.1 fusion.33
  10.0 0.3 fusion.10
  10.3 0.3 select_reduce_fusion
  10.6 0.1 select_n.104
  10.8 0.1 reshape.221
  10.9 1.5 fusion.4
  12.4 0.1 copy.75
  12.5 0.0 copy-done.1
  12.5 1.0 fusion.6
  13.5 0.1 concatenate.10
  13.6 2.3 gather_fusion
  15.9 2.4 copy_select_fusion
  18.4 32.8 %all_to_all.10 = bf16[32,8,2048]{2,0,1:T(8,128)(2,1)S(1)} all-to-all(bf16[32,8,2048]{2,0,1:T(8,128)(2,1)S(1)} %copy_select_fusion), channel_id=1, replica_groups=mesh['ep'=8,'tp'=4] {'ep'}, dimensions={1} | all-to-all | bytes 2097152 | tf_op jit(solution)/shard_map/all_to_all | solution.py:76
  51.2 1.5 copy.77
  52.7 0.0 all-gather.2.cloned.1.call-update
  52.8 0.0 reduce-scatter.2.cloned.1.call-start
  52.8 33.6 %all-gather.2.cloned.1.call-done = bf16[128,8,2048]{2,1,0:T(8,128)(2,1)} async-done(((bf16[32,8,2048]{2,1,0:T(8,128)(2,1)}), bf16[128,8,2048]{2,1,0:T(8,128)(2,1)}) %all-gather.2.cloned.1.call-update) | async-done | bytes 4194320 | tf_op jit(solution)/shard_map/all_gather | solution.py:77
  86.4 6.6 %fusion.2 = f32[1024,512]{1,0:T(8,128)} fusion(bf16[128,8,2048]{2,1,0:T(8,128)(2,1)} %all-gather.2.cloned.1.call-done, bf16[1,2048,512]{2,1,0:T(8,128)(2,1)} %param.25), kind=kOutput, calls=%fused_computation.4 | convolution fusion | flops 2147483648 | bytes 8388608 | tf_op jit(solution)/shard_map/dot_general | solution.py:79
  93.0 0.0 copy-done
  93.0 10.0 %convolution_convert_fusion = bf16[1024,2048]{1,0:T(8,128)(2,1)} fusion(bf16[1,512,2048]{2,1,0:T(8,128)(2,1)S(1)} %copy-done, f32[1024,512]{1,0:T(8,128)} %fusion.2, bf16[1,2048,512]{2,1,0:T(8,128)(2,1)} %param.26, bf16[128,8,2048]{2,1,0:T(8,128)(2,1)} %all-gather.2.cloned.1.call-done), kind=kOutput, calls=%fused_computation.8 | convolution fusion | flops 4300210176 | bytes 14680064 | tf_op jit(solution)/shard_map/dot_general | solution.py:83
  103.0 0.0 copy-start.2
  103.0 0.0 reduce-scatter.2.cloned.1.call-update
  103.0 1.0 copy-done.2
  104.0 0.2 fusion.21
  104.2 43.5 %reduce-scatter.2.cloned.1.call-done = bf16[256,2048]{1,0:T(8,128)(2,1)} async-done(((bf16[1024,2048]{1,0:T(8,128)(2,1)}), bf16[256,2048]{1,0:T(8,128)(2,1)}) %reduce-scatter.2.cloned.1.call-update) | async-done | bytes 1048592 | tf_op jit(solution)/shard_map/reduce_scatter | solution.py:82
  147.7 0.0 copy-start.3
  147.7 2.8 %copy.78 = bf16[32,8,2048]{2,0,1:T(8,128)(2,1)} copy(bf16[32,8,2048]{2,1,0:T(8,128)(2,1)} %bitcast.47) | data formatting | bytes 2097152 | tf_op jit(solution)/shard_map/reshape | solution.py:89
  150.5 5.5 %all-to-all-start.1 = ((bf16[32,8,2048]{2,0,1:T(8,128)(2,1)}), bf16[32,8,2048]{2,0,1:T(8,128)(2,1)S(1)}, u32[]{:S(2)}, u32[]{:S(2)}) async-start(bf16[32,8,2048]{2,0,1:T(8,128)(2,1)} %copy.78), calls=%async_computation.2 | async-start | bytes 2097152 | tf_op jit(solution)/shard_map/all_to_all | solution.py:88
  156.0 0.0 copy-start.4
  156.0 0.0 copy-start.5
  156.0 0.0 all-reduce.5.cloned.1.call-start
  156.1 0.0 copy-done.3
  156.1 0.0 copy-start.6
  156.1 1.7 fusion.40
  157.9 1.8 fusion.16
  159.7 4.1 %collective-permute-start = (bf16[2,256]{1,0:T(2,128)(2,1)S(1)}, bf16[2,256]{1,0:T(2,128)(2,1)S(1)}, u32[]{:S(2)}, u32[]{:S(2)}) collective-permute-start(bf16[2,256]{1,0:T(2,128)(2,1)S(1)} %slice.40), channel_id=1, source_target_pairs={{0,4},{4,8},{8,12},{12,16},{16,20},{20,24},{24,28},{1,5},{5,9},{9,... | collective-permute-start | bytes 3080 | tf_op jit(solution)/shard_map/ppermute | solution.py:10
  163.8 0.1 reshape.225
  163.9 0.1 reduce_sum.51
  164.0 0.1 copy.69
  164.1 0.0 copy-done.4
  164.2 0.0 copy-done.5
  164.2 0.2 copy.74
  164.4 0.0 copy-done.6
  164.4 0.1 copy.81
  164.5 0.3 collective-permute-done
  164.9 3.3 %convolution_convert_fusion.1 = bf16[128,2048]{1,0:T(8,128)(2,1)} fusion(bf16[256,2048]{1,0:T(8,128)(2,1)} %param.20, bf16[2048,256]{1,0:T(8,128)(2,1)} %param.18, f32[130,256]{1,0:T(8,128)S(1)} %maximum_convert_fusion, f32[256]{0:T(256)S(1)} %bitcast.51, f32[256]{0:T(256)S(1)} %bitcast.52, f32[256]{0:T(256)S(1)} %bitcast.50, bf16[128,2048]{1,0:T(8,128)(2,1)} %param.14, ...), kind=kOutput, calls=%fused_computation.11 | convolution fusion | flops 269975552 | bytes 3550720 | tf_op jit(solution)/shard_map/dot_general | solution.py:49
  168.2 13.5 %all-to-all-done.1 = bf16[32,8,2048]{2,0,1:T(8,128)(2,1)S(1)} async-done(((bf16[32,8,2048]{2,0,1:T(8,128)(2,1)}), bf16[32,8,2048]{2,0,1:T(8,128)(2,1)S(1)}, u32[]{:S(2)}, u32[]{:S(2)}) %all-to-all-start.1) | async-done | bytes 1048608 | tf_op jit(solution)/shard_map/all_to_all | solution.py:88
  181.7 0.6 copy.84
  182.3 0.1 concatenate.11
  182.4 3.3 %gather_fusion.1 = bf16[512,2048]{1,0:T(8,128)(2,1)} fusion(bf16[257,2048]{1,0:T(8,128)(2,1)S(1)} %concatenate.11, s32[1024]{0:T(1024)S(1)} %pad_clamp_fusion), kind=kCustom, calls=%fused_computation.1 | custom fusion | bytes 4196352 | tf_op jit(solution)/shard_map/jit(_take)/gather | solution.py:108
  185.7 4.4 %gather.15 = bf16[256,2,2048]{2,1,0:T(2,128)(2,1)} reshape(bf16[512,2048]{1,0:T(8,128)(2,1)} %gather_fusion.1) | data formatting | bytes 4194304 | tf_op jit(solution)/shard_map/jit(_take)/gather | solution.py:108
  190.1 10.8 %multiply_reduce_fusion = bf16[256,2048]{1,0:T(8,128)(2,1)} fusion(bf16[256,2,2048]{2,1,0:T(2,128)(2,1)} %gather.15, pred[256,2]{1,0:T(8,128)(4,1)S(1)} %copy.74, f32[256,2]{1,0:T(8,128)S(1)} %copy.81), kind=kLoop, calls=%fused_computation.6 | loop fusion | flops 3670016 | bytes 3148288 | tf_op jit(solution)/shard_map/reduce_sum | solution.py:111
  201.0 0.0 all-reduce.5.cloned.1.call-update
  201.0 43.5 %all-reduce.5.cloned.1.call-done = (bf16[128,2048]{1,0:T(8,128)(2,1)}, bf16[256,2048]{1,0:T(8,128)(2,1)}) async-done(((bf16[128,2048]{1,0:T(8,128)(2,1)}, bf16[256,2048]{1,0:T(8,128)(2,1)}), (bf16[128,2048]{1,0:T(8,128)(2,1)}, bf16[256,2048]{1,0:T(8,128)(2,1)})) %all-reduce.5.cloned.1.call-update) | async-done | bytes 1572880 | tf_op jit(solution)/shard_map/psum | solution.py:113
  244.5 1.9 copy.87
  246.4 2.3 copy.88
  (16 shorter events, 0.2 us)
Async XLA Ops:
  7.2 85.8 %copy-start = (bf16[1,512,2048]{2,1,0:T(8,128)(2,1)S(1)}, bf16[1,512,2048]{2,1,0:T(8,128)(2,1)}, u32[]{:S(2)}) copy-start(bf16[1,512,2048]{2,1,0:T(8,128)(2,1)} %param.27) | copy-start | bytes 6291460
  7.2 5.3 %copy-start.1 = (bf16[256,2048]{1,0:T(8,128)(2,1)S(1)}, bf16[256,2048]{1,0:T(8,128)(2,1)}, u32[]{:S(2)}) copy-start(bf16[256,2048]{1,0:T(8,128)(2,1)} %param.21) | copy-start | bytes 3145732
  7.2 79.2 %all-gather.2.cloned.1.call-start = ((), (), s32[]{:S(2)}) async-start(), calls=%async_computation.3 | async-start | bytes 5242880 | tf_op jit(solution)/shard_map/all_gather | solution.py:77
  52.8 95.0 %reduce-scatter.2.cloned.1.call-start = ((), (), s32[]{:S(2)}) async-start(), calls=%async_computation.4 | async-start | bytes 5242880 | tf_op jit(solution)/shard_map/reduce_scatter | solution.py:82
  103.0 1.0 copy-start.2
  147.7 8.4 %copy-start.3 = (f32[2048]{0:T(1024)S(1)}, f32[2048]{0:T(1024)}, u32[]{:S(2)}) copy-start(f32[2048]{0:T(1024)} %param.15) | copy-start | bytes 24580
  150.5 31.2 %all-to-all-start.1 = ((bf16[32,8,2048]{2,0,1:T(8,128)(2,1)}), bf16[32,8,2048]{2,0,1:T(8,128)(2,1)S(1)}, u32[]{:S(2)}, u32[]{:S(2)}) async-start(bf16[32,8,2048]{2,0,1:T(8,128)(2,1)} %copy.78), calls=%async_computation.2 | async-start | bytes 2097152 | tf_op jit(solution)/shard_map/all_to_all | solution.py:88
  156.0 8.1 %copy-start.4 = (s32[256,2]{0,1:T(2,128)S(1)}, s32[256,2]{0,1:T(2,128)}, u32[]{:S(2)}) copy-start(s32[256,2]{0,1:T(2,128)} %param.23) | copy-start | bytes 6148
  156.0 8.1 %copy-start.5 = (f32[3,256]{1,0:T(4,128)S(1)}, f32[3,256]{1,0:T(4,128)}, u32[]{:S(2)}) copy-start(f32[3,256]{1,0:T(4,128)} %param.19) | copy-start | bytes 9220
  156.0 88.4 %all-reduce.5.cloned.1.call-start = ((), (), s32[]{:S(2)}) async-start(), calls=%async_computation.5 | async-start | bytes 3145728 | tf_op jit(solution)/shard_map/psum | solution.py:113
  156.1 8.3 %copy-start.6 = (f32[256,2]{0,1:T(2,128)S(1)}, f32[256,2]{0,1:T(2,128)}, u32[]{:S(2)}) copy-start(f32[256,2]{0,1:T(2,128)} %param.24) | copy-start | bytes 6148
  159.7 5.2 %collective-permute-start = (bf16[2,256]{1,0:T(2,128)(2,1)S(1)}, bf16[2,256]{1,0:T(2,128)(2,1)S(1)}, u32[]{:S(2)}, u32[]{:S(2)}) collective-permute-start(bf16[2,256]{1,0:T(2,128)(2,1)S(1)} %slice.40), channel_id=1, source_target_pairs={{0,4},{4,8},{8,12},{12,16},{16,20},{20,24},{24,28},{1,5},{5,9},{9,... | collective-permute-start | bytes 3080 | tf_op jit(solution)/shard_map/ppermute | solution.py:10
Sparse Core Ops, SparseCore 0:
  52.9 33.4 all-gather.1
  103.1 44.5 reduce-scatter.1
  201.1 43.3 all-reduce.4
where the time goes:
time: 256 us; the launch traced here: 255 us
  waiting for transfers between devices  134 us (52%)
  blocking collectives  32.8 us (13%)
  matrix products  23.4 us (9%)
  local copies, waits for them, and re-layouts  22.8 us (9%)
  other arithmetic  18 us (7%)
  between operations  14 us (5%)
  starting transfers between devices  9.73 us (4%)
    reduce_scatter x1, waiting for transfers between devices, on_device(): lax.psum_scatter(jnp.dot(hidden, expert_down[0], preferred_element_type=j...  43.5 us
    psum x1, waiting for transfers between devices, on_device(): lax.psum(mixer_terms.astype(jnp.bfloat16), 'tp').astype(jnp.float32)  43.5 us
    all_gather x1, waiting for transfers between devices, on_device(): incoming = lax.all_gather(arrived, 'tp', axis=0, tiled=True)  33.6 us
    all_to_all x1, blocking collectives, on_device(): lax.all_to_all(outgoing, 'ep', split_axis=1, concat_axis=1, tiled=True)  32.8 us
    all_to_all x1, waiting for transfers between devices, on_device(): lax.all_to_all(summed.reshape(share_rows, experts, model_width), 'ep', sp...  13.5 us
    reduce_sum x1, other arithmetic, on_device(): jnp.sum(contrib.reshape(tok_count, pick_count, model_width), axis=1)  10.8 us
    dot_general x1, matrix products, on_device(): jnp.dot(hidden, expert_down[0], preferred_element_type=jnp.float32)  9.96 us
    gather x2, local copies, waits for them, and re-layouts, on_device(): jnp.take(flat_back, local_slot, axis=0).astype(jnp.float32)  7.75 us
  transfers between devices with their start and end apart: 5, of which 5 were waited for; matrix products, arithmetic and copies ran while one was open for 3% of the time, Pallas kernels for 0%

commit v1 on v0

--- a/solution.py
+++ b/solution.py
@@ -2,6 +2,17 @@
 import jax.numpy as jnp
 from jax import lax
 from jax.sharding import PartitionSpec as P
+
+
+def _find_tables(own_rows, d0, dim_no):
+    right_arr = lax.all_to_all(
+        jnp.stack(jnp.split(own_rows, lax.psum(1, axis_name="ep"), axis=d0)),
+        axis_name="ep",
+        split_axis=0,
+        concat_axis=0,
+    )
+    outer = jnp.concatenate(right_arr, axis=dim_no)
+    return outer
 
 
 def shifted(value, axis, steps):
@@ -85,13 +96,7 @@
         scatter_dimension=0,
         tiled=True,
     )
-    returned = lax.all_to_all(
-        summed.reshape(share_rows, experts, model_width),
-        "ep",
-        split_axis=1,
-        concat_axis=1,
-        tiled=True,
-    )
+    returned = _find_tables(summed.reshape(share_rows, experts, model_width), 1, 1)
     flat_back = jnp.concatenate(
         [
             returned.reshape(share_rows * experts, model_width),

time: 256 us -> 265 us (1.035)
  local copies, waits for them, and re-layouts: 22.8 us -> 32.4 us
    split x0 -> x1, local copies, waits for them, and re-layouts: none -> 6.5 us  [_find_tables(): jnp.split(own_rows, lax.psum(1, axis_name='ep'), axis=d0)]
    unnamed x18 -> x25, local copies, waits for them, and re-layouts: 6.36 us -> 11.5 us
where the time goes in v1:
time: 265 us
  waiting for transfers between devices  135 us (51%)
  blocking collectives  32.8 us (12%)
  local copies, waits for them, and re-layouts  32.4 us (12%)
  matrix products  23.4 us (9%)
  other arithmetic  18 us (7%)
  between operations  14 us (5%)
  starting transfers between devices  9.55 us (4%)
    reduce_scatter x1, waiting for transfers between devices, on_device(): lax.psum_scatter(jnp.dot(hidden, expert_down[0], preferred_element_type=j...  43.5 us
    psum x1, waiting for transfers between devices, on_device(): lax.psum(mixer_terms.astype(jnp.bfloat16), 'tp').astype(jnp.float32)  43.5 us
    all_gather x1, waiting for transfers between devices, on_device(): incoming = lax.all_gather(arrived, 'tp', axis=0, tiled=True)  33.6 us
    all_to_all x1, blocking collectives, on_device(): lax.all_to_all(outgoing, 'ep', split_axis=1, concat_axis=1, tiled=True)  32.8 us
    all_to_all x1, waiting for transfers between devices, _find_tables(): lax.all_to_all(jnp.stack(jnp.split(own_rows, lax.psum(1, axis_name='ep'),...  13.5 us
    unnamed x25, local copies, waits for them, and re-layouts  11.5 us
    reduce_sum x1, other arithmetic, on_device(): jnp.sum(contrib.reshape(tok_count, pick_count, model_width), axis=1)  10.8 us
    dot_general x1, matrix products, on_device(): jnp.dot(hidden, expert_down[0], preferred_element_type=jnp.float32)  9.96 us
  transfers between devices with their start and end apart: 5, of which 5 were waited for; matrix products, arithmetic and copies ran while one was open for 3% of the time, Pallas kernels for 0%

profile of v1, /device:TPU:0, one launch (start us, length us, event | category | flops | bytes accessed | tf_op | source)
XLA Modules:
  0.0 264.8 jit_solution(17510317270379526477)
XLA Ops:
  7.2 0.0 copy-start
  7.2 0.0 copy-start.1
  7.2 0.0 all-gather.2.cloned.1.call-start
  7.2 1.0 copy.98
  8.2 0.1 eq.62
  8.4 0.1 eq.58
  8.5 1.1 reduce-window.6
  9.7 0.2 slice_reduce_fusion
  9.9 0.1 fusion.41
  10.0 0.3 fusion.10
  10.3 0.3 select_reduce_fusion
  10.6 0.1 select_n.104
  10.8 0.1 reshape.221
  10.9 1.5 fusion.4
  12.4 0.1 copy.106
  12.5 1.0 fusion.6
  13.5 0.1 concatenate.10
  13.6 2.3 gather_fusion
  15.9 2.4 copy_select_fusion
  18.4 32.8 %all_to_all.10 = bf16[32,8,2048]{2,0,1:T(8,128)(2,1)S(1)} all-to-all(bf16[32,8,2048]{2,0,1:T(8,128)(2,1)S(1)} %copy_select_fusion), channel_id=1, replica_groups=mesh['ep'=8,'tp'=4] {'ep'}, dimensions={1} | all-to-all | bytes 2097152 | tf_op jit(solution)/shard_map/all_to_all | solution.py:87
  51.2 1.5 copy.108
  52.7 0.0 all-gather.2.cloned.1.call-update
  52.8 0.0 reduce-scatter.2.cloned.1.call-start
  52.8 33.6 %all-gather.2.cloned.1.call-done = bf16[128,8,2048]{2,1,0:T(8,128)(2,1)} async-done(((bf16[32,8,2048]{2,1,0:T(8,128)(2,1)}), bf16[128,8,2048]{2,1,0:T(8,128)(2,1)}) %all-gather.2.cloned.1.call-update) | async-done | bytes 4194320 | tf_op jit(solution)/shard_map/all_gather | solution.py:88
  86.4 6.6 %fusion.2 = f32[1024,512]{1,0:T(8,128)} fusion(bf16[128,8,2048]{2,1,0:T(8,128)(2,1)} %all-gather.2.cloned.1.call-done, bf16[1,2048,512]{2,1,0:T(8,128)(2,1)} %param.25), kind=kOutput, calls=%fused_computation.4 | convolution fusion | flops 2147483648 | bytes 8388608 | tf_op jit(solution)/shard_map/dot_general | solution.py:90
  93.0 10.0 %convolution_convert_fusion = bf16[1024,2048]{1,0:T(8,128)(2,1)} fusion(bf16[1,512,2048]{2,1,0:T(8,128)(2,1)S(1)} %copy-done, f32[1024,512]{1,0:T(8,128)} %fusion.2, bf16[1,2048,512]{2,1,0:T(8,128)(2,1)} %param.26, bf16[128,8,2048]{2,1,0:T(8,128)(2,1)} %all-gather.2.cloned.1.call-done), kind=kOutput, calls=%fused_computation.8 | convolution fusion | flops 4300210176 | bytes 14680064 | tf_op jit(solution)/shard_map/dot_general | solution.py:94
  103.0 0.0 reduce-scatter.2.cloned.1.call-update
  103.0 1.0 copy-done.2
  104.0 0.2 fusion.21
  104.2 43.5 %reduce-scatter.2.cloned.1.call-done = bf16[256,2048]{1,0:T(8,128)(2,1)} async-done(((bf16[1024,2048]{1,0:T(8,128)(2,1)}), bf16[256,2048]{1,0:T(8,128)(2,1)}) %reduce-scatter.2.cloned.1.call-update) | async-done | bytes 1048592 | tf_op jit(solution)/shard_map/reduce_scatter | solution.py:93
  147.7 6.5 %fusion.52 = (bf16[32,1,2048]{2,1,0:T(2,128)(2,1)S(1)}, bf16[32,1,2048]{2,1,0:T(2,128)(2,1)S(1)}, bf16[32,1,2048]{2,1,0:T(2,128)(2,1)S(1)}, bf16[32,1,2048]{2,1,...) fusion(bf16[32,8,2048]{2,1,0:T(8,128)(2,1)} %bitcast.81), kind=kLoop, calls=%fused_computation.98 | loop fusion | bytes 2097152 | tf_op jit(solution)/shard_map/split | solution.py:9
  154.2 0.7 fusion.36
  155.0 0.7 fusion.35
  155.7 0.7 fusion.34
  156.5 0.7 fusion.33
  157.2 0.7 fusion.32
  157.9 0.7 fusion.31
  158.7 0.7 fusion.30
  159.4 0.7 fusion.29
  160.1 5.5 %all-to-all-start.1 = ((bf16[8,32,1,2048]{3,1,2,0:T(8,128)(2,1)}), bf16[8,32,1,2048]{3,1,2,0:T(8,128)(2,1)S(1)}, u32[]{:S(2)}, u32[]{:S(2)}) async-start(bf16[8,32,1,2048]{3,1,2,0:T(8,128)(2,1)} %fusion.29), calls=%async_computation.2 | async-start | bytes 2097152 | tf_op jit(solution)/shard_map/all_to_all | solution.py:8
  165.7 0.0 copy-start.5
  165.7 0.0 all-reduce.5.cloned.1.call-start
  165.7 0.0 copy-start.6
  165.8 1.7 fusion.48
  167.5 1.7 fusion.16
  169.3 3.9 %collective-permute-start = (bf16[2,256]{1,0:T(2,128)(2,1)S(1)}, bf16[2,256]{1,0:T(2,128)(2,1)S(1)}, u32[]{:S(2)}, u32[]{:S(2)}) collective-permute-start(bf16[2,256]{1,0:T(2,128)(2,1)S(1)} %slice.40), channel_id=1, source_target_pairs={{0,4},{4,8},{8,12},{12,16},{16,20},{20,24},{24,28},{1,5},{5,9},{9,... | collective-permute-start | bytes 3080 | tf_op jit(solution)/shard_map/ppermute | solution.py:21
  173.2 0.1 reshape.225
  173.3 0.1 reduce_sum.51
  173.5 0.1 copy.100
  173.7 0.2 copy.105
  173.8 0.0 copy-done.6
  173.9 0.1 copy.119
  174.0 0.5 collective-permute-done
  174.5 3.3 %convolution_convert_fusion.1 = bf16[128,2048]{1,0:T(8,128)(2,1)} fusion(bf16[256,2048]{1,0:T(8,128)(2,1)} %param.20, bf16[2048,256]{1,0:T(8,128)(2,1)} %param.18, f32[130,256]{1,0:T(8,128)S(1)} %maximum_convert_fusion, f32[256]{0:T(256)S(1)} %bitcast.85, f32[256]{0:T(256)S(1)} %bitcast.86, f32[256]{0:T(256)S(1)} %bitcast.84, bf16[128,2048]{1,0:T(8,128)(2,1)} %param.14, ...), kind=kOutput, calls=%fused_computation.11 | convolution fusion | flops 269975552 | bytes 3550720 | tf_op jit(solution)/shard_map/dot_general | solution.py:60
  177.8 13.5 %all-to-all-done.1 = bf16[8,32,1,2048]{3,1,2,0:T(8,128)(2,1)S(1)} async-done(((bf16[8,32,1,2048]{3,1,2,0:T(8,128)(2,1)}), bf16[8,32,1,2048]{3,1,2,0:T(8,128)(2,1)S(1)}, u32[]{:S(2)}, u32[]{:S(2)}) %all-to-all-start.1) | async-done | bytes 1048608 | tf_op jit(solution)/shard_map/all_to_all | solution.py:8
  191.3 0.6 copy.154
  191.9 0.1 concatenate.11
  192.0 3.3 %gather_fusion.1 = bf16[512,2048]{1,0:T(8,128)(2,1)} fusion(bf16[257,2048]{1,0:T(8,128)(2,1)S(1)} %concatenate.11, s32[1024]{0:T(1024)S(1)} %pad_clamp_fusion), kind=kCustom, calls=%fused_computation.1 | custom fusion | bytes 4196352 | tf_op jit(solution)/shard_map/jit(_take)/gather | solution.py:113
  195.3 4.4 %gather.15 = bf16[256,2,2048]{2,1,0:T(2,128)(2,1)} reshape(bf16[512,2048]{1,0:T(8,128)(2,1)} %gather_fusion.1) | data formatting | bytes 4194304 | tf_op jit(solution)/shard_map/jit(_take)/gather | solution.py:113
  199.7 10.8 %multiply_reduce_fusion = bf16[256,2048]{1,0:T(8,128)(2,1)} fusion(bf16[256,2,2048]{2,1,0:T(2,128)(2,1)} %gather.15, pred[256,2]{1,0:T(8,128)(4,1)S(1)} %copy.105, f32[256,2]{1,0:T(8,128)S(1)} %copy.119), kind=kLoop, calls=%fused_computation.6 | loop fusion | flops 3670016 | bytes 3148288 | tf_op jit(solution)/shard_map/reduce_sum | solution.py:116
  210.6 0.0 all-reduce.5.cloned.1.call-update
  210.6 43.5 %all-reduce.5.cloned.1.call-done = (bf16[128,2048]{1,0:T(8,128)(2,1)}, bf16[256,2048]{1,0:T(8,128)(2,1)}) async-done(((bf16[128,2048]{1,0:T(8,128)(2,1)}, bf16[256,2048]{1,0:T(8,128)(2,1)}), (bf16[128,2048]{1,0:T(8,128)(2,1)}, bf16[256,2048]{1,0:T(8,128)(2,1)})) %all-reduce.5.cloned.1.call-update) | async-done | bytes 1572880 | tf_op jit(solution)/shard_map/psum | solution.py:118
  254.1 1.9 copy.164
  256.0 2.3 copy.165
  (24 shorter events, 0.2 us)
Async XLA Ops:
  7.2 85.8 %copy-start = (bf16[1,512,2048]{2,1,0:T(8,128)(2,1)S(1)}, bf16[1,512,2048]{2,1,0:T(8,128)(2,1)}, u32[]{:S(2)}) copy-start(bf16[1,512,2048]{2,1,0:T(8,128)(2,1)} %param.27) | copy-start | bytes 6291460
  7.2 5.3 %copy-start.1 = (bf16[256,2048]{1,0:T(8,128)(2,1)S(1)}, bf16[256,2048]{1,0:T(8,128)(2,1)}, u32[]{:S(2)}) copy-start(bf16[256,2048]{1,0:T(8,128)(2,1)} %param.21) | copy-start | bytes 3145732
  7.2 79.2 %all-gather.2.cloned.1.call-start = ((), (), s32[]{:S(2)}) async-start(), calls=%async_computation.3 | async-start | bytes 5242880 | tf_op jit(solution)/shard_map/all_gather | solution.py:88
  52.8 95.0 %reduce-scatter.2.cloned.1.call-start = ((), (), s32[]{:S(2)}) async-start(), calls=%async_computation.4 | async-start | bytes 5242880 | tf_op jit(solution)/shard_map/reduce_scatter | solution.py:93
  103.0 1.0 copy-start.2
  156.4 9.3 %copy-start.3 = (f32[2048]{0:T(1024)S(1)}, f32[2048]{0:T(1024)}, u32[]{:S(2)}) copy-start(f32[2048]{0:T(1024)} %param.15) | copy-start | bytes 24580
  160.1 31.2 %all-to-all-start.1 = ((bf16[8,32,1,2048]{3,1,2,0:T(8,128)(2,1)}), bf16[8,32,1,2048]{3,1,2,0:T(8,128)(2,1)S(1)}, u32[]{:S(2)}, u32[]{:S(2)}) async-start(bf16[8,32,1,2048]{3,1,2,0:T(8,128)(2,1)} %fusion.29), calls=%async_computation.2 | async-start | bytes 2097152 | tf_op jit(solution)/shard_map/all_to_all | solution.py:8
  165.7 7.9 %copy-start.4 = (s32[256,2]{0,1:T(2,128)S(1)}, s32[256,2]{0,1:T(2,128)}, u32[]{:S(2)}) copy-start(s32[256,2]{0,1:T(2,128)} %param.23) | copy-start | bytes 6148
  165.7 8.0 %copy-start.5 = (f32[3,256]{1,0:T(4,128)S(1)}, f32[3,256]{1,0:T(4,128)}, u32[]{:S(2)}) copy-start(f32[3,256]{1,0:T(4,128)} %param.19) | copy-start | bytes 9220
  165.7 88.4 %all-reduce.5.cloned.1.call-start = ((), (), s32[]{:S(2)}) async-start(), calls=%async_computation.5 | async-start | bytes 3145728 | tf_op jit(solution)/shard_map/psum | solution.py:118
  165.7 8.1 %copy-start.6 = (f32[256,2]{0,1:T(2,128)S(1)}, f32[256,2]{0,1:T(2,128)}, u32[]{:S(2)}) copy-start(f32[256,2]{0,1:T(2,128)} %param.24) | copy-start | bytes 6148
  169.3 5.2 %collective-permute-start = (bf16[2,256]{1,0:T(2,128)(2,1)S(1)}, bf16[2,256]{1,0:T(2,128)(2,1)S(1)}, u32[]{:S(2)}, u32[]{:S(2)}) collective-permute-start(bf16[2,256]{1,0:T(2,128)(2,1)S(1)} %slice.40), channel_id=1, source_target_pairs={{0,4},{4,8},{8,12},{12,16},{16,20},{20,24},{24,28},{1,5},{5,9},{9,... | collective-permute-start | bytes 3080 | tf_op jit(solution)/shard_map/ppermute | solution.py:21
Sparse Core Ops, SparseCore 0:
  52.9 33.4 all-gather.1
  103.1 44.5 reduce-scatter.1
  210.7 43.3 all-reduce.4
